TPU v7x, 32 devices: a whole 2x2x4 slice. The times are simulated.
32 devices in a mesh: ep: 8 (over z, x), tp: 4 (over y, core).
Axes of the slice: x: 2, y: 2, z: 4, core: 2. Of those that a mesh axis runs over, the one named last changes fastest.
Arguments:
- tokens: bfloat16 [256, 2048], P('ep'), may hold values from -6 to 6
- norm_gain: float32 [2048], replicated, may hold values from 0.1 to 1.9
- norm_bias: float32 [2048], replicated, may hold values from -3 to 3
- routes: int32 [256, 4], P('ep'), may hold values from 0 to 7, all different within a row; in each aligned block of 32 rows (0 to 31, 32 to 63, ...) at most 32 rows name the same one
- route_weights: float32 [256, 4], P('ep'), may hold values from 0.2 to 1
- gate_w: bfloat16 [8, 2048, 4096], P('ep', None, 'tp'), may hold values from -0.125 to 0.125
- up_w: bfloat16 [8, 2048, 4096], P('ep', None, 'tp'), may hold values from -0.125 to 0.125
- down_w: bfloat16 [8, 4096, 2048], P('ep', 'tp'), may hold values from -0.09375 to 0.09375
Outputs:
- mixed: bfloat16 [256, 2048], P('ep', 'tp')
Inputs may be any that keep to these rules, and one draw needn't show every extreme that they name: `routes`: the 4 experts of a token differ; the rows of one index of ep name no expert more than 32 times, and in every draw some index of ep names some expert exactly 32 times.
All inputs are finite; a program needn't handle non-finite values.
Results may differ from a plain program's by a relative error of at most 0.017.
Values may be sent and summed in bfloat16 or wider, within the bound.
No kernel may reach another device: no remote copies, remote signals or barrier semaphores. Data moves between devices by JAX's collectives and lax.ppermute only.
A program may use at most 64 MiB of HBM per device.

v0:
```python
import jax
import jax.numpy as jnp
from jax import lax
from jax.sharding import PartitionSpec as P


def layer_norm(tokens, norm_gain, norm_bias):
    values = tokens.astype(jnp.float32)
    centred = values - jnp.mean(values, axis=-1, keepdims=True)
    variance = jnp.mean(centred * centred, axis=-1, keepdims=True)
    return (centred * lax.rsqrt(variance + 1e-05) * norm_gain + norm_bias).astype(jnp.bfloat16)


def body(tokens, norm_gain, norm_bias, routes, route_weights, gate_w, up_w, down_w):
    tok_rows, width = tokens.shape
    topk = routes.shape[1]
    experts = lax.axis_size("ep")
    capacity = 2 * tok_rows * topk // experts
    normed = layer_norm(tokens, norm_gain, norm_bias)
    flat_routes = routes.reshape(-1)
    onehot = (flat_routes[:, None] == jnp.arange(experts, dtype=jnp.int32)[None, :]).astype(
        jnp.int32
    )
    ranks = jnp.sum((jnp.cumsum(onehot, axis=0) - onehot) * onehot, axis=1)
    slots = flat_routes * capacity + ranks
    placed = slots[:, None] == jnp.arange(experts * capacity, dtype=jnp.int32)[None, :]
    picker = jnp.any(placed.reshape(tok_rows, topk, experts * capacity), axis=1).T.astype(
        jnp.bfloat16
    )
    outgoing = jnp.dot(picker, normed, preferred_element_type=jnp.float32).astype(jnp.bfloat16)
    outgoing = outgoing.reshape(experts, capacity, width)
    received = lax.all_to_all(outgoing, "ep", split_axis=0, concat_axis=0, tiled=True)
    sources, items, _ = received.shape
    flat_rows = received.reshape(sources * items, width)
    gate = jnp.dot(flat_rows, gate_w[0], preferred_element_type=jnp.float32)
    up = jnp.dot(flat_rows, up_w[0], preferred_element_type=jnp.float32)
    hidden = (jax.nn.silu(gate) * up).astype(jnp.bfloat16)
    partial_value = jnp.dot(hidden, down_w[0], preferred_element_type=jnp.float32)
    partial_value = partial_value.astype(jnp.bfloat16).astype(jnp.float32)
    summed = lax.psum_scatter(
        partial_value.astype(jnp.bfloat16), "tp", scatter_dimension=1, tiled=True
    )
    produced = summed.reshape(sources, items, summed.shape[1])
    returned = lax.all_to_all(produced, "ep", split_axis=0, concat_axis=0, tiled=True)
    returned = returned.reshape(experts * capacity, returned.shape[2])
    routed = jnp.dot(placed.astype(jnp.bfloat16), returned, preferred_element_type=jnp.float32)
    routed = routed.reshape(tok_rows, topk, routed.shape[1])
    result = jnp.sum(route_weights[:, :, None] * routed, axis=1)
    return result.astype(jnp.bfloat16)


def solution(mesh):
    placed = (
        P("ep", None),
        P(),
        P(),
        P("ep", None),
        P("ep", None),
        P("ep", None, "tp"),
        P("ep", None, "tp"),
        P("ep", "tp", None),
    )
    return jax.shard_map(body, mesh=mesh, in_specs=placed, out_specs=P("ep", "tp"), check_vma=False)
```

profile of v0, /device:TPU:0, one launch (start us, length us, event | category | flops | bytes accessed | tf_op | source)
XLA Modules:
  0.0 101.8 jit_solution(15928419642523925810)
XLA Ops:
  6.5 0.0 reduce-scatter.2.cloned.1.call-start
  6.5 1.0 %convert_reduce_fusion = f32[32]{0:T(128)S(1)} fusion(bf16[32,2048]{1,0:T(8,128)(2,1)} %param.8), kind=kLoop, calls=%fused_computation.14 | loop fusion | flops 131040 | bytes 131200 | tf_op jit(solution)/shard_map/reduce_sum | solution.py:9
  7.6 1.1 %fusion.21 = f32[32]{0:T(128)S(1)} fusion(bf16[32,2048]{1,0:T(8,128)(2,1)} %param.8, f32[32]{0:T(128)S(1)} %broadcast_multiply_fusion), kind=kLoop, calls=%fused_computation.17 | loop fusion | flops 262112 | bytes 131328 | tf_op jit(solution)/shard_map/reduce_sum | solution.py:10
  8.7 0.8 copy.22
  9.5 0.1 eq.51
  9.6 0.1 fusion.34
  9.7 0.2 reduce_window_sum.11
  9.8 0.2 select_reduce_fusion
  10.0 0.1 reduce_sum.39
  10.1 0.1 copy.23
  10.2 0.7 multiply_add_fusion
  10.9 0.1 fusion.32
  11.0 1.4 %convolution_convert_fusion = bf16[256,2048]{1,0:T(8,128)(2,1)S(1)} fusion(pred[32,256]{1,0:T(8,128)(4,1)S(1)} %fusion.32, bf16[32,2048]{1,0:T(8,128)(2,1)} %param.8, f32[2048]{0:T(1024)} %param.10, f32[2048]{0:T(1024)} %param.9, f32[32]{0:T(128)S(1)} %add_rsqrt_fusion, f32[32]{0:T(128)S(1)} %broadcast_multiply_fusion), kind=kOutput, calls=%fused_computation.7 | convolution fusion | flops 34471936 | bytes 1204480 | tf_op jit(solution)/shard_map/dot_general | solution.py:30
  12.4 32.8 %all_to_all.10 = bf16[8,32,2048]{2,1,0:T(8,128)(2,1)S(1)} all-to-all(bf16[8,32,2048]{2,1,0:T(8,128)(2,1)S(1)} %bitcast.30), channel_id=1, replica_groups=mesh['ep'=8,'tp'=4] {'ep'}, dimensions={0} | all-to-all | bytes 2097152 | tf_op jit(solution)/shard_map/all_to_all | solution.py:32
  45.3 3.5 %fusion.4 = f32[256,1024]{1,0:T(8,128)S(1)} fusion(bf16[256,2048]{1,0:T(8,128)(2,1)S(1)} %bitcast.31, bf16[1,2048,1024]{2,1,0:T(8,128)(2,1)} %param.13), kind=kOutput, calls=%fused_computation.4 | convolution fusion | flops 1073741824 | bytes 6291456 | tf_op jit(solution)/shard_map/dot_general | solution.py:35
  48.8 0.0 copy-start
  48.8 7.0 %fusion.6 = bf16[256,2048]{1,0:T(8,128)(2,1)} fusion(bf16[1,1024,2048]{2,1,0:T(8,128)(2,1)} %param.15, bf16[256,2048]{1,0:T(8,128)(2,1)S(1)} %bitcast.32, bf16[1,2048,1024]{2,1,0:T(8,128)(2,1)} %param.14, f32[256,1024]{1,0:T(8,128)S(1)} %fusion.4), kind=kOutput, calls=%fused_computation.6 | convolution fusion | flops 2149580800 | bytes 11534336 | tf_op jit(solution)/shard_map/dot_general | solution.py:38
  55.8 0.0 reduce-scatter.2.cloned.1.call-update
  55.8 24.0 %reduce-scatter.2.cloned.1.call-done = bf16[256,512]{1,0:T(8,128)(2,1)} async-done(((bf16[256,2048]{1,0:T(8,128)(2,1)}), bf16[256,512]{1,0:T(8,128)(2,1)}) %reduce-scatter.2.cloned.1.call-update) | async-done | bytes 262160 | tf_op jit(solution)/shard_map/reduce_scatter | solution.py:40
  79.8 14.3 %all_to_all.11 = bf16[8,32,512]{2,1,0:T(8,128)(2,1)S(1)} all-to-all(bf16[8,32,512]{2,1,0:T(8,128)(2,1)} %bitcast.33), channel_id=1, replica_groups=mesh['ep'=8,'tp'=4] {'ep'}, dimensions={0} | all-to-all | bytes 524288 | tf_op jit(solution)/shard_map/all_to_all | solution.py:44
  94.1 0.0 copy-done
  94.1 0.8 fusion.15
  (2 shorter events, 0.0 us)
Async XLA Ops:
  6.5 73.3 %reduce-scatter.2.cloned.1.call-start = ((), (), s32[]{:S(2)}) async-start(), calls=%async_computation.3 | async-start | bytes 1310720 | tf_op jit(solution)/shard_map/reduce_scatter | solution.py:40
  48.8 45.3 %copy-start = (f32[32,4]{0,1:T(4,128)S(1)}, f32[32,4]{0,1:T(4,128)}, u32[]{:S(2)}) copy-start(f32[32,4]{0,1:T(4,128)} %param.12) | copy-start | bytes 1540
Sparse Core Ops, SparseCore 0:
  55.9 23.8 reduce-scatter.1
where the time goes:
time: 102 us
  blocking collectives  47.1 us (46%)
  waiting for transfers between devices  24 us (24%)
  between operations  13.4 us (13%)
  matrix products  12.8 us (13%)
  other arithmetic  3.38 us (3%)
  local copies, waits for them, and re-layouts  1.06 us (1%)
    all_to_all x1, blocking collectives, body(): lax.all_to_all(outgoing, 'ep', split_axis=0, concat_axis=0, tiled=True)  32.8 us
    reduce_scatter x1, waiting for transfers between devices, body(): lax.psum_scatter(partial_value.astype(jnp.bfloat16), 'tp', scatter_dimens...  24 us
    all_to_all x1, blocking collectives, body(): lax.all_to_all(produced, 'ep', split_axis=0, concat_axis=0, tiled=True)  14.3 us
    dot_general x1, matrix products, body(): jnp.dot(hidden, down_w[0], preferred_element_type=jnp.float32)  7.03 us
    dot_general x1, matrix products, body(): gate = jnp.dot(flat_rows, gate_w[0], preferred_element_type=jnp.float32)  3.46 us
  transfers between devices with their start and end apart: 1, of which 1 were waited for; matrix products, arithmetic and copies ran while one was open for 0% of the time, Pallas kernels for 0%

commit v1 on v0

v1 whole, which is shorter than its diff:
```python
import functools

import jax
import jax.numpy as jnp
from jax import lax
from jax.experimental import pallas as pl
from jax.experimental.pallas import tpu as pltpu
from jax.sharding import PartitionSpec as P


AXES = ("ep", "tp")
CORES = 2
LANES = 128


class Grid:
    def __init__(self, ep, tp):
        self.y = tp // CORES
        self.x = self.y
        self.z = ep // self.x
        assert self.z * self.x == ep and self.y * CORES == tp
        self.devices = ep * tp

    def place(self, device):
        rest, core = divmod(device, CORES)
        rest, y = divmod(rest, self.y)
        z, x = divmod(rest, self.x)
        return z, x, y, core

    def device(self, z, x, y, core):
        return ((z * self.x + x) * self.y + y) * CORES + core

    def permute(self, value, moves):
        pairs = []
        for source in range(self.devices):
            here = self.place(source)
            move = moves[here[3]]
            if move is not None:
                pairs.append((source, self.device(*(a ^ b for a, b in zip(here, move)))))
        return lax.ppermute(value, AXES, pairs)


def in_hbm(value):
    return pltpu.with_memory_space_constraint(value, pltpu.HBM)


def fetch_kernel(*refs):
    count = len(refs) // 2
    sems = refs[-1]
    copies = [pltpu.make_async_copy(refs[i], refs[count + i], sems.at[i]) for i in range(count)]
    for copy in copies:
        copy.start()
    for copy in copies:
        copy.wait()


def prepare_kernel(*refs):
    out_ref, sems = refs[5], refs[11]
    copies = [pltpu.make_async_copy(refs[i], refs[6 + i], sems.at[i]) for i in range(5)]
    for copy in copies:
        copy.start()
    for copy in copies:
        copy.wait()
    tokens_ref, gain_ref, bias_ref, routes_ref, weights_ref = refs[6:11]
    values = tokens_ref[...].astype(jnp.float32)
    rows, width = values.shape
    centred = values - jnp.mean(values, axis=-1, keepdims=True)
    variance = jnp.mean(centred * centred, axis=-1, keepdims=True)
    normed = centred * lax.rsqrt(variance + 1e-05) * gain_ref[...] + bias_ref[...]
    out_ref[:, :width] = normed.astype(jnp.bfloat16)
    half = LANES // 2
    expert = lax.broadcasted_iota(jnp.int32, (half, rows), 0)
    total = jnp.zeros((half, rows), jnp.float32)
    for k in range(routes_ref.shape[0]):
        total += jnp.where(routes_ref[k : k + 1, :] == expert, weights_ref[k : k + 1, :], 0.0)
    high = total.astype(jnp.bfloat16)
    low = (total - high.astype(jnp.float32)).astype(jnp.bfloat16)
    lane = lax.broadcasted_iota(jnp.int32, (half, LANES), 1)
    line = lax.broadcasted_iota(jnp.int32, (half, LANES), 0)
    marks = jnp.zeros((rows, LANES), jnp.float32)
    for value, shift in ((high, 0), (low, half)):
        spread = (lane == line + shift).astype(jnp.bfloat16)
        marks += lax.dot_general(
            value, spread, (((0,), (0,)), ((), ())), preferred_element_type=jnp.float32
        )
    out_ref[:, width:] = marks.astype(jnp.bfloat16)


def expert_kernel(grid, pairs, chunk, *refs):
    count = 1 + 2 * len(pairs)
    blocks = refs[:count]
    gate_ref, up_ref, down_ref, keep_ref, send_ref, rows_ref, hidden_ref = refs[count:]
    width, units = gate_ref.shape[1:]
    columns = keep_ref.shape[-1]
    tok_rows = blocks[0].shape[0]

    core = lax.axis_index("tp") % CORES
    expert = lax.axis_index("ep")
    spare = grid.z * grid.x

    def slot(message):
        return spare if message is None else message[1] * grid.z + message[0]

    def place(block, at):
        start = pl.multiple_of(at * tok_rows, tok_rows)
        rows_ref[pl.ds(start, tok_rows), :] = block[...]

    place(blocks[0], 0)
    for i, (first, second) in enumerate(pairs):
        place(blocks[1 + 2 * i], jnp.where(core == 0, slot(first), slot(second)))
        place(blocks[2 + 2 * i], jnp.where(core == 0, slot(second), slot(first)))

    total_rows = spare * tok_rows
    for step in range(units // chunk):
        part = slice(step * chunk, (step + 1) * chunk)
        normed = rows_ref[:total_rows, :width]
        gate = jnp.dot(normed, gate_ref[0, :, part], preferred_element_type=jnp.float32)
        up = jnp.dot(normed, up_ref[0, :, part], preferred_element_type=jnp.float32)
        hidden_ref[:, part] = (gate / (1.0 + jnp.exp(-gate)) * up).astype(jnp.bfloat16)

    marks = rows_ref[:total_rows, width:].astype(jnp.float32)
    lane = lax.broadcasted_iota(jnp.int32, marks.shape, 1)
    mine = (lane == expert) | (lane == expert + LANES // 2)
    scale = jnp.sum(jnp.where(mine, marks, 0.0), axis=-1, keepdims=True)

    side = grid.z * tok_rows
    for y in range(grid.y):
        for c in range(CORES):
            owner = lax.axis_index("tp") ^ (y * CORES + c)
            start = pl.multiple_of(owner * columns, columns)
            part = jnp.dot(
                hidden_ref[...],
                down_ref[0, :, pl.ds(start, columns)],
                preferred_element_type=jnp.float32,
            )
            part = (part * scale).astype(jnp.bfloat16)
            target = send_ref if c else keep_ref
            y_first = core == c
            for x in range(grid.x):
                a = jnp.where(y_first, y, x)
                b = jnp.where(y_first, x, y)
                target[a, b] = part[x * side : (x + 1) * side]


def body(grid, tokens, norm_gain, norm_bias, routes, route_weights, gate_w, up_w, down_w):
    tok_rows, width = tokens.shape
    experts = lax.axis_size("ep")
    units = gate_w.shape[2]
    columns = width // lax.axis_size("tp")
    sources = (tokens, norm_gain[None, :], norm_bias[None, :], routes.T, route_weights.T)
    block = pl.pallas_call(
        prepare_kernel,
        out_shape=jax.ShapeDtypeStruct((tok_rows, width + LANES), jnp.bfloat16),
        in_specs=[pl.BlockSpec(memory_space=pltpu.HBM)] * 5,
        out_specs=pl.BlockSpec(memory_space=pltpu.VMEM),
        scratch_shapes=[pltpu.VMEM(a.shape, a.dtype) for a in sources]
        + [pltpu.SemaphoreType.DMA((5,))],
        compiler_params=pltpu.CompilerParams(vmem_limit_bytes=4 << 20),
        name="prepare",
    )(*map(in_hbm, sources))

    direct = [(z, 0) for z in range(2, grid.z)] + [(1, 0)] * (grid.z > 1)
    direct += [(0, x) for x in range(1, grid.x)]
    direct += [(1, x) for x in range(1, grid.x)] * (grid.z > 1)
    onward = [(z, x) for x in range(1, grid.x) for z in range(2, grid.z)]
    pairs, got = [], []
    for messages in (direct, onward):
        for first, second in zip(messages[::2], messages[1::2] + [None] * (len(messages) % 2)):
            pair = (first, second)
            if messages is direct:
                got.append(grid.permute(block, [m and (*m, 0, 0) for m in pair]))
            else:
                held = got[pairs.index(((first[0], 0), second and (second[0], 0)))]
                got.append(grid.permute(held, [m and (0, m[1], 0, 0) for m in pair]))
            pairs.append(pair)
    blocks = [block]
    for held in got:
        blocks += [held, grid.permute(held, [(0, 0, 0, 1)] * CORES)]

    weights = (gate_w, up_w, down_w)
    load = pl.pallas_call(
        fetch_kernel,
        out_shape=[pltpu.VMEM(w.shape, w.dtype) for w in weights],
        in_specs=[pl.BlockSpec(memory_space=pltpu.HBM)] * len(weights),
        out_specs=[pl.BlockSpec(memory_space=pltpu.VMEM)] * len(weights),
        scratch_shapes=[pltpu.SemaphoreType.DMA((len(weights),))],
        compiler_params=pltpu.CompilerParams(vmem_limit_bytes=1 << 20),
        name="fetch",
    )
    gate_w, up_w, down_w = load(*map(in_hbm, weights))

    rows = experts * tok_rows
    chunk = 256
    shape = (grid.y, grid.x, grid.z * tok_rows, columns)
    keep, send = pl.pallas_call(
        functools.partial(expert_kernel, grid, pairs, chunk),
        out_shape=[jax.ShapeDtypeStruct(shape, jnp.bfloat16)] * 2,
        in_specs=[pl.BlockSpec(memory_space=pltpu.VMEM)] * (len(blocks) + 3),
        out_specs=[pl.BlockSpec(memory_space=pltpu.VMEM)] * 2,
        scratch_shapes=[
            pltpu.VMEM((rows + tok_rows, width + LANES), jnp.bfloat16),
            pltpu.VMEM((rows, units), jnp.bfloat16),
        ],
        compiler_params=pltpu.CompilerParams(vmem_limit_bytes=24 << 20),
        name="expert",
    )(*blocks, gate_w, up_w, down_w)

    def add(*parts):
        total = parts[0].astype(jnp.float32)
        for part in parts[1:]:
            total = total + part.astype(jnp.float32)
        return total.astype(jnp.bfloat16)

    held = add(keep, grid.permute(send, [(0, 0, 0, 1)] * CORES))
    held = add(
        held[0],
        *(grid.permute(held[i], [(0, 0, i, 0), (0, i, 0, 0)]) for i in range(1, grid.y)),
    )
    held = add(
        held[0],
        *(grid.permute(held[i], [(0, i, 0, 0), (0, 0, i, 0)]) for i in range(1, grid.x)),
    )
    held = held.reshape(grid.z, tok_rows, columns)
    return add(
        held[0],
        *(grid.permute(held[i], [(i, 0, 0, 0)] * CORES) for i in range(1, grid.z)),
    )


def solution(mesh):
    grid = Grid(mesh.shape["ep"], mesh.shape["tp"])
    placed = (
        P("ep", None),
        P(),
        P(),
        P("ep", None),
        P("ep", None),
        P("ep", None, "tp"),
        P("ep", None, "tp"),
        P("ep", "tp", None),
    )
    return jax.shard_map(
        functools.partial(body, grid),
        mesh=mesh,
        in_specs=placed,
        out_specs=P("ep", "tp"),
        check_vma=False,
    )
```

time: 102 us -> 48.2 us (0.47)
  blocking collectives: 47.1 us -> 0 us
  starting transfers between devices: 0.01 us -> 18 us
  between operations: 13.4 us -> 0.11 us
  matrix products: 12.8 us -> 0 us
  Pallas kernels: 0 us -> 9.51 us
  waiting for transfers between devices: 24 us -> 19.6 us
  other arithmetic: 3.38 us -> 0.87 us
  local copies, waits for them, and re-layouts: 1.06 us -> 0.04 us
    all_to_all x2 -> x0, blocking collectives: 47.1 us -> none  [the longest x1 32.8 us: body(): lax.all_to_all(outgoing, 'ep', split_axis=0, concat_axis=0, tiled=True)]
    reduce_scatter x1 -> x0, waiting for transfers between devices: 24 us -> none  [body(): lax.psum_scatter(partial_value.astype(jnp.bfloat16), 'tp', scatter_dimens...]
    ppermute x0 -> x14, waiting for transfers between devices: none -> 19.6 us  [permute(): return lax.ppermute(value, AXES, pairs)]
    ppermute x0 -> x14, starting transfers between devices: none -> 18 us  [permute(): return lax.ppermute(value, AXES, pairs)]
    dot_general x4 -> x0, matrix products: 12.8 us -> none  [the longest x1 7.03 us: body(): jnp.dot(hidden, down_w[0], preferred_element_type=jnp.float32)]
    pallas_call x0 -> x3, Pallas kernels: none -> 9.51 us  [the longest x1 4.69 us: body(): gate_w, up_w, down_w = load(*map(in_hbm, weights))]
    reduce_sum x3 -> x0, other arithmetic: 2.32 us -> none  [the longest x1 1.12 us: layer_norm(): variance = jnp.mean(centred * centred, axis=-1, keepdims=True)]
  transfers between devices with their start and end apart: 1 -> 14, of which waited for: 1 -> 10; matrix products, arithmetic and copies ran while one was open for 0% -> 0% of each run, Pallas kernels for 0% -> 10%
where the time goes in v1:
time: 48.2 us; the launch traced here: 48.1 us
  waiting for transfers between devices  19.6 us (41%)
  starting transfers between devices  18 us (37%)
  Pallas kernels  9.51 us (20%)
  other arithmetic  0.87 us (2%)
    ppermute x14, waiting for transfers between devices, permute(): return lax.ppermute(value, AXES, pairs)  19.6 us
    ppermute x14, starting transfers between devices, permute(): return lax.ppermute(value, AXES, pairs)  18 us
    pallas_call x1, Pallas kernels, body(): gate_w, up_w, down_w = load(*map(in_hbm, weights))  4.69 us
    pallas_call x1, Pallas kernels, body(): pl.pallas_call(functools.partial(expert_kernel, grid, pairs, chunk), out_...  3.62 us
    pallas_call x1, Pallas kernels, body(): pl.pallas_call(prepare_kernel, out_shape=jax.ShapeDtypeStruct((tok_rows,...  1.21 us
  transfers between devices with their start and end apart: 14, of which 10 were waited for; matrix products, arithmetic and copies ran while one was open for 0% of the time, Pallas kernels for 10%

profile of v1, /device:TPU:0, one launch (start us, length us, event | category | flops | bytes accessed | tf_op | source)
XLA Modules:
  0.0 48.1 jit_solution(17454879887019409440)
XLA Ops:
  0.0 1.2 %prepare.1.refs_0_ = bf16[32,2176]{1,0:T(8,128)(2,1)S(1)} custom-call(bf16[32,2048]{1,0:T(8,128)(2,1)} %refs_0_.2, f32[1,2048]{1,0:T(1,128)} %bitcast.18, f32[1,2048]{1,0:T(1,128)} %bitcast.19, s32[4,32]{1,0:T(4,128)} %bitcast.20, f32[4,32]{1,0:T(4,128)} %bitcast.21), custom_call_target="tpu_custom_call" | custom-call | tf_op jit(solution)/shard_map/prepare/pallas_call | solution.py:151
  1.2 4.1 %collective-permute-start = (bf16[32,2176]{1,0:T(8,128)(2,1)S(1)}, bf16[32,2176]{1,0:T(8,128)(2,1)S(1)}, u32[]{:S(2)}, u32[]{:S(2)}) collective-permute-start(bf16[32,2176]{1,0:T(8,128)(2,1)S(1)} %prepare.1.refs_0_), channel_id=1, source_target_pairs={{0,16},{1,25},{2,18},{3,27},{4,20},{5,29},{6,22},{7,31},{8,24},{9,... | collective-permute-start | bytes 417800 | tf_op jit(solution)/shard_map/ppermute | solution.py:40
  5.3 4.4 %collective-permute-start.4 = (bf16[32,2176]{1,0:T(8,128)(2,1)S(1)}, bf16[32,2176]{1,0:T(8,128)(2,1)S(1)}, u32[]{:S(2)}, u32[]{:S(2)}) collective-permute-start(bf16[32,2176]{1,0:T(8,128)(2,1)S(1)} %prepare.1.refs_0_), channel_id=1, source_target_pairs={{0,12},{2,14},{4,8},{6,10},{8,4},{10,6},{12,0},{14,2},{16,28},{18,... | collective-permute-start | bytes 417800 | tf_op jit(solution)/shard_map/ppermute | solution.py:40
  9.8 0.5 %collective-permute-start.2 = (bf16[32,2176]{1,0:T(8,128)(2,1)S(1)}, bf16[32,2176]{1,0:T(8,128)(2,1)S(1)}, u32[]{:S(2)}, u32[]{:S(2)}) collective-permute-start(bf16[32,2176]{1,0:T(8,128)(2,1)S(1)} %prepare.1.refs_0_), channel_id=1, source_target_pairs={{0,8},{1,5},{2,10},{3,7},{4,12},{5,1},{6,14},{7,3},{8,0},{9,13},{1... | collective-permute-start | bytes 417800 | tf_op jit(solution)/shard_map/ppermute | solution.py:40
  10.3 1.9 %collective-permute-done.refs_1_ = bf16[32,2176]{1,0:T(8,128)(2,1)S(1)} collective-permute-done((bf16[32,2176]{1,0:T(8,128)(2,1)S(1)}, bf16[32,2176]{1,0:T(8,128)(2,1)S(1)}, u32[]{:S(2)}, u32[]{:S(2)}) %collective-permute-start) | collective-permute-done | bytes 139296 | tf_op jit(solution)/shard_map/ppermute | solution.py:40
  12.2 1.5 %collective-permute-start.6 = (bf16[32,2176]{1,0:T(8,128)(2,1)S(1)}, bf16[32,2176]{1,0:T(8,128)(2,1)S(1)}, u32[]{:S(2)}, u32[]{:S(2)}) collective-permute-start(bf16[32,2176]{1,0:T(8,128)(2,1)S(1)} %collective-permute-done.refs_1_), channel_id=1, source_target_pairs={{0,4},{1,5},{2,6},{3,7},{4,0},{5,1},{6,2},{7,3},{8,12},{9,13},{10,... | collective-permute-start | bytes 417800 | tf_op jit(solution)/shard_map/ppermute | solution.py:40
  13.8 0.0 collective-permute-start.1
  13.8 0.7 %collective-permute-done.4.refs_5_ = bf16[32,2176]{1,0:T(8,128)(2,1)S(1)} collective-permute-done((bf16[32,2176]{1,0:T(8,128)(2,1)S(1)}, bf16[32,2176]{1,0:T(8,128)(2,1)S(1)}, u32[]{:S(2)}, u32[]{:S(2)}) %collective-permute-start.4) | collective-permute-done | bytes 139296 | tf_op jit(solution)/shard_map/ppermute | solution.py:40
  14.5 0.0 collective-permute-start.5
  14.5 0.7 %collective-permute-done.2.refs_3_ = bf16[32,2176]{1,0:T(8,128)(2,1)S(1)} collective-permute-done((bf16[32,2176]{1,0:T(8,128)(2,1)S(1)}, bf16[32,2176]{1,0:T(8,128)(2,1)S(1)}, u32[]{:S(2)}, u32[]{:S(2)}) %collective-permute-start.2) | collective-permute-done | bytes 139296 | tf_op jit(solution)/shard_map/ppermute | solution.py:40
  15.2 0.0 collective-permute-start.3
  15.2 2.1 %collective-permute-done.6.refs_7_ = bf16[32,2176]{1,0:T(8,128)(2,1)S(1)} collective-permute-done((bf16[32,2176]{1,0:T(8,128)(2,1)S(1)}, bf16[32,2176]{1,0:T(8,128)(2,1)S(1)}, u32[]{:S(2)}, u32[]{:S(2)}) %collective-permute-start.6) | collective-permute-done | bytes 139296 | tf_op jit(solution)/shard_map/ppermute | solution.py:40
  17.3 0.0 collective-permute-start.7
  17.3 4.7 %fetch.1 = (bf16[1,2048,1024]{2,1,0:T(8,128)(2,1)S(1)}, bf16[1,2048,1024]{2,1,0:T(8,128)(2,1)S(1)}, bf16[1,1024,2048]{2,1,0:T(8,128)(2,1)S(1)}) custom-call(bf16[1,2048,1024]{2,1,0:T(8,128)(2,1)} %refs_0_.3, bf16[1,2048,1024]{2,1,0:T(8,128)(2,1)} %refs_1_.1, bf16[1,1024,2048]{2,1,0:T(8,128)(2,1)} %refs_2_.1), custom_call_target="tpu_custom_call" | custom-call | tf_op jit(solution)/shard_map/fetch/pallas_call | solution.py:190
  22.0 0.0 collective-permute-done.5.refs_6_
  22.0 0.0 collective-permute-done.3.refs_4_
  22.0 0.0 collective-permute-done.1.refs_2_
  22.0 0.0 collective-permute-done.7.refs_8_
  22.0 3.6 %expert.1 = (bf16[2,2,128,512]{3,2,1,0:T(8,128)(2,1)S(1)}, bf16[2,2,128,512]{3,2,1,0:T(8,128)(2,1)S(1)}) custom-call(bf16[32,2176]{1,0:T(8,128)(2,1)S(1)} %prepare.1.refs_0_, bf16[32,2176]{1,0:T(8,128)(2,1)S(1)} %collective-permute-done.refs_1_, bf16[32,2176]{1,0:T(8,128)(2,1)S(1)} %collective-permute-done.1.refs_2_, ...), custom_call_target="tpu_custom_call" | custom-call | tf_op jit(solution)/shard_map/expert/pallas_call | solution.py:195
  25.6 0.6 %collective-permute-start.8 = (bf16[2,2,128,512]{3,2,1,0:T(8,128)(2,1)S(1)}, bf16[2,2,128,512]{3,2,1,0:T(8,128)(2,1)S(1)}, u32[]{:S(2)}, u32[]{:S(2)}) collective-permute-start(bf16[2,2,128,512]{3,2,1,0:T(8,128)(2,1)S(1)} %get-tuple-element.14), channel_id=1, source_target_pairs={{0,1},{1,0},{2,3},{3,2},{4,5},{5,4},{6,7},{7,6},{8,9},{9,8},{10,11... | collective-permute-start | bytes 1572872 | tf_op jit(solution)/shard_map/ppermute | solution.py:40
  26.2 1.5 %collective-permute-done.8 = bf16[2,2,128,512]{3,2,1,0:T(8,128)(2,1)S(1)} collective-permute-done((bf16[2,2,128,512]{3,2,1,0:T(8,128)(2,1)S(1)}, bf16[2,2,128,512]{3,2,1,0:T(8,128)(2,1)S(1)}, u32[]{:S(2)}, u32[]{:S(2)}) %collective-permute-start.8) | collective-permute-done | bytes 524320 | tf_op jit(solution)/shard_map/ppermute | solution.py:40
  27.7 0.1 add_convert_fusion
  27.9 1.6 %collective-permute-start.9 = (bf16[2,128,512]{2,1,0:T(8,128)(2,1)S(1)}, bf16[2,128,512]{2,1,0:T(8,128)(2,1)S(1)}, u32[]{:S(2)}, u32[]{:S(2)}) collective-permute-start(bf16[2,128,512]{2,1,0:T(8,128)(2,1)S(1)} %slice_bitcast_fusion), channel_id=1, source_target_pairs={{0,2},{1,5},{2,0},{3,7},{4,6},{5,1},{6,4},{7,3},{8,10},{9,13},{10,... | collective-permute-start | bytes 786440 | tf_op jit(solution)/shard_map/ppermute | solution.py:40
  29.5 4.9 %collective-permute-done.9 = bf16[2,128,512]{2,1,0:T(8,128)(2,1)S(1)} collective-permute-done((bf16[2,128,512]{2,1,0:T(8,128)(2,1)S(1)}, bf16[2,128,512]{2,1,0:T(8,128)(2,1)S(1)}, u32[]{:S(2)}, u32[]{:S(2)}) %collective-permute-start.9) | collective-permute-done | bytes 262176 | tf_op jit(solution)/shard_map/ppermute | solution.py:40
  34.3 0.1 fusion
  34.4 1.6 %collective-permute-start.10 = (bf16[128,512]{1,0:T(8,128)(2,1)S(1)}, bf16[128,512]{1,0:T(8,128)(2,1)S(1)}, u32[]{:S(2)}, u32[]{:S(2)}) collective-permute-start(bf16[128,512]{1,0:T(8,128)(2,1)S(1)} %slice_bitcast_fusion.2), channel_id=1, source_target_pairs={{0,4},{1,3},{2,6},{3,1},{4,0},{5,7},{6,2},{7,5},{8,12},{9,11},{10,... | collective-permute-start | bytes 393224 | tf_op jit(solution)/shard_map/ppermute | solution.py:40
  36.1 3.4 %collective-permute-done.10 = bf16[128,512]{1,0:T(8,128)(2,1)S(1)} collective-permute-done((bf16[128,512]{1,0:T(8,128)(2,1)S(1)}, bf16[128,512]{1,0:T(8,128)(2,1)S(1)}, u32[]{:S(2)}, u32[]{:S(2)}) %collective-permute-start.10) | collective-permute-done | bytes 131104 | tf_op jit(solution)/shard_map/ppermute | solution.py:40
  39.5 0.5 %collective-permute-start.11 = (bf16[32,512]{1,0:T(8,128)(2,1)S(1)}, bf16[32,512]{1,0:T(8,128)(2,1)S(1)}, u32[]{:S(2)}, u32[]{:S(2)}) collective-permute-start(bf16[32,512]{1,0:T(8,128)(2,1)S(1)} %get-tuple-element.15), channel_id=1, source_target_pairs={{0,8},{1,9},{2,10},{3,11},{4,12},{5,13},{6,14},{7,15},{8,0},{9,1},... | collective-permute-start | bytes 98312 | tf_op jit(solution)/shard_map/ppermute | solution.py:40
  40.1 2.5 %collective-permute-start.13 = (bf16[32,512]{1,0:T(8,128)(2,1)S(1)}, bf16[32,512]{1,0:T(8,128)(2,1)S(1)}, u32[]{:S(2)}, u32[]{:S(2)}) collective-permute-start(bf16[32,512]{1,0:T(8,128)(2,1)S(1)} %get-tuple-element.16), channel_id=1, source_target_pairs={{0,24},{1,25},{2,26},{3,27},{4,28},{5,29},{6,30},{7,31},{8,16},{9,... | collective-permute-start | bytes 98312 | tf_op jit(solution)/shard_map/ppermute | solution.py:40
  42.6 0.5 %collective-permute-start.12 = (bf16[32,512]{1,0:T(8,128)(2,1)S(1)}, bf16[32,512]{1,0:T(8,128)(2,1)S(1)}, u32[]{:S(2)}, u32[]{:S(2)}) collective-permute-start(bf16[32,512]{1,0:T(8,128)(2,1)S(1)} %get-tuple-element.17), channel_id=1, source_target_pairs={{0,16},{1,17},{2,18},{3,19},{4,20},{5,21},{6,22},{7,23},{8,24},{9,... | collective-permute-start | bytes 98312 | tf_op jit(solution)/shard_map/ppermute | solution.py:40
  43.1 0.4 collective-permute-done.11
  43.5 2.3 %collective-permute-done.13 = bf16[32,512]{1,0:T(8,128)(2,1)S(1)} collective-permute-done((bf16[32,512]{1,0:T(8,128)(2,1)S(1)}, bf16[32,512]{1,0:T(8,128)(2,1)S(1)}, u32[]{:S(2)}, u32[]{:S(2)}) %collective-permute-start.13) | collective-permute-done | bytes 32800 | tf_op jit(solution)/shard_map/ppermute | solution.py:40
  45.8 1.6 %collective-permute-done.12 = bf16[32,512]{1,0:T(8,128)(2,1)S(1)} collective-permute-done((bf16[32,512]{1,0:T(8,128)(2,1)S(1)}, bf16[32,512]{1,0:T(8,128)(2,1)S(1)}, u32[]{:S(2)}, u32[]{:S(2)}) %collective-permute-start.12) | collective-permute-done | bytes 32800 | tf_op jit(solution)/shard_map/ppermute | solution.py:40
  47.4 0.6 %add_convert_fusion.1 = bf16[32,512]{1,0:T(8,128)(2,1)} fusion(bf16[32,512]{1,0:T(8,128)(2,1)S(1)} %collective-permute-done.13, bf16[32,512]{1,0:T(8,128)(2,1)S(1)} %collective-permute-done.12, bf16[32,512]{1,0:T(8,128)(2,1)S(1)} %collective-permute-done.11, bf16[128,512]{1,0:T(8,128)(2,1)S(1)} %fusion.1), kind=kLoop, calls=%fused_computation.9 | loop fusion | flops 131072 | bytes 163840 | tf_op jit(solution)/shard_map/convert_element_type | solution.py:212
  (4 shorter events, 0.1 us)
Async XLA Ops:
  1.2 11.0 %collective-permute-start = (bf16[32,2176]{1,0:T(8,128)(2,1)S(1)}, bf16[32,2176]{1,0:T(8,128)(2,1)S(1)}, u32[]{:S(2)}, u32[]{:S(2)}) collective-permute-start(bf16[32,2176]{1,0:T(8,128)(2,1)S(1)} %prepare.1.refs_0_), channel_id=1, source_target_pairs={{0,16},{1,25},{2,18},{3,27},{4,20},{5,29},{6,22},{7,31},{8,24},{9,... | collective-permute-start | bytes 417800 | tf_op jit(solution)/shard_map/ppermute | solution.py:40
  5.3 9.1 %collective-permute-start.4 = (bf16[32,2176]{1,0:T(8,128)(2,1)S(1)}, bf16[32,2176]{1,0:T(8,128)(2,1)S(1)}, u32[]{:S(2)}, u32[]{:S(2)}) collective-permute-start(bf16[32,2176]{1,0:T(8,128)(2,1)S(1)} %prepare.1.refs_0_), channel_id=1, source_target_pairs={{0,12},{2,14},{4,8},{6,10},{8,4},{10,6},{12,0},{14,2},{16,28},{18,... | collective-permute-start | bytes 417800 | tf_op jit(solution)/shard_map/ppermute | solution.py:40
  9.8 5.4 %collective-permute-start.2 = (bf16[32,2176]{1,0:T(8,128)(2,1)S(1)}, bf16[32,2176]{1,0:T(8,128)(2,1)S(1)}, u32[]{:S(2)}, u32[]{:S(2)}) collective-permute-start(bf16[32,2176]{1,0:T(8,128)(2,1)S(1)} %prepare.1.refs_0_), channel_id=1, source_target_pairs={{0,8},{1,5},{2,10},{3,7},{4,12},{5,1},{6,14},{7,3},{8,0},{9,13},{1... | collective-permute-start | bytes 417800 | tf_op jit(solution)/shard_map/ppermute | solution.py:40
  12.2 5.1 %collective-permute-start.6 = (bf16[32,2176]{1,0:T(8,128)(2,1)S(1)}, bf16[32,2176]{1,0:T(8,128)(2,1)S(1)}, u32[]{:S(2)}, u32[]{:S(2)}) collective-permute-start(bf16[32,2176]{1,0:T(8,128)(2,1)S(1)} %collective-permute-done.refs_1_), channel_id=1, source_target_pairs={{0,4},{1,5},{2,6},{3,7},{4,0},{5,1},{6,2},{7,3},{8,12},{9,13},{10,... | collective-permute-start | bytes 417800 | tf_op jit(solution)/shard_map/ppermute | solution.py:40
  13.8 8.2 %collective-permute-start.1 = (bf16[32,2176]{1,0:T(8,128)(2,1)S(1)}, bf16[32,2176]{1,0:T(8,128)(2,1)S(1)}, u32[]{:S(2)}, u32[]{:S(2)}) collective-permute-start(bf16[32,2176]{1,0:T(8,128)(2,1)S(1)} %collective-permute-done.refs_1_), channel_id=1, source_target_pairs={{0,1},{1,0},{2,3},{3,2},{4,5},{5,4},{6,7},{7,6},{8,9},{9,8},{10,11... | collective-permute-start | bytes 417800 | tf_op jit(solution)/shard_map/ppermute | solution.py:40
  14.5 7.5 %collective-permute-start.5 = (bf16[32,2176]{1,0:T(8,128)(2,1)S(1)}, bf16[32,2176]{1,0:T(8,128)(2,1)S(1)}, u32[]{:S(2)}, u32[]{:S(2)}) collective-permute-start(bf16[32,2176]{1,0:T(8,128)(2,1)S(1)} %collective-permute-done.4.refs_5_), channel_id=1, source_target_pairs={{0,1},{1,0},{2,3},{3,2},{4,5},{5,4},{6,7},{7,6},{8,9},{9,8},{10,11... | collective-permute-start | bytes 417800 | tf_op jit(solution)/shard_map/ppermute | solution.py:40
  15.2 6.8 %collective-permute-start.3 = (bf16[32,2176]{1,0:T(8,128)(2,1)S(1)}, bf16[32,2176]{1,0:T(8,128)(2,1)S(1)}, u32[]{:S(2)}, u32[]{:S(2)}) collective-permute-start(bf16[32,2176]{1,0:T(8,128)(2,1)S(1)} %collective-permute-done.2.refs_3_), channel_id=1, source_target_pairs={{0,1},{1,0},{2,3},{3,2},{4,5},{5,4},{6,7},{7,6},{8,9},{9,8},{10,11... | collective-permute-start | bytes 417800 | tf_op jit(solution)/shard_map/ppermute | solution.py:40
  17.3 4.7 %collective-permute-start.7 = (bf16[32,2176]{1,0:T(8,128)(2,1)S(1)}, bf16[32,2176]{1,0:T(8,128)(2,1)S(1)}, u32[]{:S(2)}, u32[]{:S(2)}) collective-permute-start(bf16[32,2176]{1,0:T(8,128)(2,1)S(1)} %collective-permute-done.6.refs_7_), channel_id=1, source_target_pairs={{0,1},{1,0},{2,3},{3,2},{4,5},{5,4},{6,7},{7,6},{8,9},{9,8},{10,11... | collective-permute-start | bytes 417800 | tf_op jit(solution)/shard_map/ppermute | solution.py:40
  25.6 2.1 %collective-permute-start.8 = (bf16[2,2,128,512]{3,2,1,0:T(8,128)(2,1)S(1)}, bf16[2,2,128,512]{3,2,1,0:T(8,128)(2,1)S(1)}, u32[]{:S(2)}, u32[]{:S(2)}) collective-permute-start(bf16[2,2,128,512]{3,2,1,0:T(8,128)(2,1)S(1)} %get-tuple-element.14), channel_id=1, source_target_pairs={{0,1},{1,0},{2,3},{3,2},{4,5},{5,4},{6,7},{7,6},{8,9},{9,8},{10,11... | collective-permute-start | bytes 1572872 | tf_op jit(solution)/shard_map/ppermute | solution.py:40
  27.9 6.4 %collective-permute-start.9 = (bf16[2,128,512]{2,1,0:T(8,128)(2,1)S(1)}, bf16[2,128,512]{2,1,0:T(8,128)(2,1)S(1)}, u32[]{:S(2)}, u32[]{:S(2)}) collective-permute-start(bf16[2,128,512]{2,1,0:T(8,128)(2,1)S(1)} %slice_bitcast_fusion), channel_id=1, source_target_pairs={{0,2},{1,5},{2,0},{3,7},{4,6},{5,1},{6,4},{7,3},{8,10},{9,13},{10,... | collective-permute-start | bytes 786440 | tf_op jit(solution)/shard_map/ppermute | solution.py:40
  34.4 5.0 %collective-permute-start.10 = (bf16[128,512]{1,0:T(8,128)(2,1)S(1)}, bf16[128,512]{1,0:T(8,128)(2,1)S(1)}, u32[]{:S(2)}, u32[]{:S(2)}) collective-permute-start(bf16[128,512]{1,0:T(8,128)(2,1)S(1)} %slice_bitcast_fusion.2), channel_id=1, source_target_pairs={{0,4},{1,3},{2,6},{3,1},{4,0},{5,7},{6,2},{7,5},{8,12},{9,11},{10,... | collective-permute-start | bytes 393224 | tf_op jit(solution)/shard_map/ppermute | solution.py:40
  39.5 4.0 %collective-permute-start.11 = (bf16[32,512]{1,0:T(8,128)(2,1)S(1)}, bf16[32,512]{1,0:T(8,128)(2,1)S(1)}, u32[]{:S(2)}, u32[]{:S(2)}) collective-permute-start(bf16[32,512]{1,0:T(8,128)(2,1)S(1)} %get-tuple-element.15), channel_id=1, source_target_pairs={{0,8},{1,9},{2,10},{3,11},{4,12},{5,13},{6,14},{7,15},{8,0},{9,1},... | collective-permute-start | bytes 98312 | tf_op jit(solution)/shard_map/ppermute | solution.py:40
  40.1 5.7 %collective-permute-start.13 = (bf16[32,512]{1,0:T(8,128)(2,1)S(1)}, bf16[32,512]{1,0:T(8,128)(2,1)S(1)}, u32[]{:S(2)}, u32[]{:S(2)}) collective-permute-start(bf16[32,512]{1,0:T(8,128)(2,1)S(1)} %get-tuple-element.16), channel_id=1, source_target_pairs={{0,24},{1,25},{2,26},{3,27},{4,28},{5,29},{6,30},{7,31},{8,16},{9,... | collective-permute-start | bytes 98312 | tf_op jit(solution)/shard_map/ppermute | solution.py:40
  42.6 4.8 %collective-permute-start.12 = (bf16[32,512]{1,0:T(8,128)(2,1)S(1)}, bf16[32,512]{1,0:T(8,128)(2,1)S(1)}, u32[]{:S(2)}, u32[]{:S(2)}) collective-permute-start(bf16[32,512]{1,0:T(8,128)(2,1)S(1)} %get-tuple-element.17), channel_id=1, source_target_pairs={{0,16},{1,17},{2,18},{3,19},{4,20},{5,21},{6,22},{7,23},{8,24},{9,... | collective-permute-start | bytes 98312 | tf_op jit(solution)/shard_map/ppermute | solution.py:40
